TPU v7x, 256 devices: a whole 4x4x8 slice. The times are simulated.
256 devices in a mesh: sp: 64 (over z, x, core), tp: 4 (over y).
Axes of the slice: x: 4, y: 4, z: 8, core: 2. Of those that a mesh axis runs over, the one named last changes fastest.
Arguments:
- residual_in: bfloat16 [65536, 2048], P(('sp', 'tp')), may hold values from -6 to 6
- gate_outer: bfloat16 [65536, 1024], P('sp', 'tp'), may hold values from -6 to 6
- gate_inner: bfloat16 [65536, 1024], P('sp', 'tp'), may hold values from -6 to 6
- conv_input: bfloat16 [65536, 1024], P('sp', 'tp'), may hold values from -6 to 6
- conv_taps: bfloat16 [3, 1024], P(None, 'tp'), may hold values from -5 to 5
- norm_gain: bfloat16 [1024], P('tp'), may hold values from 0.099609375 to 1.8984375
- out_weight: bfloat16 [1024, 2048], P('tp'), may hold values from -0.1875 to 0.1875
- moe_gain: bfloat16 [2048], replicated, may hold values from 0.099609375 to 1.8984375
- expert_ids: int32 [65536, 2], P(('sp', 'tp')), may hold values from 0 to 63, all different within a row; in each aligned block of 256 rows (0 to 255, 256 to 511, ...) at most 16 rows name the same one
- group_prob: float32 [65536], P(('sp', 'tp')), may hold values from 0.3 to 1
- route_prob: float32 [65536, 2], P(('sp', 'tp')), may hold values from 0.1 to 1
- expert_gate: bfloat16 [64, 2048, 512], P('sp'), may hold values from -0.125 to 0.125
- expert_up: bfloat16 [64, 2048, 512], P('sp'), may hold values from -0.125 to 0.125
- expert_down: bfloat16 [64, 512, 2048], P('sp'), may hold values from -0.25 to 0.25
Outputs:
- layer_out: bfloat16 [65536, 2048], P(('sp', 'tp'))
Inputs may be any that keep to these rules, and one draw needn't show every extreme that they name: `expert_ids`: each row names 2 different experts. Within the rows of one device (aligned blocks of 256 rows) no expert is named more than 16 times.
All inputs are finite; a program needn't handle non-finite values.
Results may differ from a plain program's by a relative error of at most 0.0075.
Values may be sent and summed in bfloat16 or wider, within the bound.
A program may use at most 64 MiB of HBM per device.

v0:
```python
import jax
import jax.numpy as jnp
from jax import lax
from jax.sharding import PartitionSpec as P

EPSILON = 1e-06


def from_behind(shard, axis, by):
    devices = lax.axis_size(axis)
    pairs = [(i, i + by) for i in range(devices) if 0 <= i + by < devices]
    return lax.ppermute(shard, axis, pairs)


def rms_norm(values, gain):
    floats = values.astype(jnp.float32)
    factor = lax.rsqrt(jnp.mean(floats * floats, axis=-1, keepdims=True) + EPSILON)
    return floats * factor * gain.astype(jnp.float32)


def body(
    residual_in,
    gate_outer,
    gate_inner,
    conv_input,
    conv_taps,
    norm_gain,
    out_weight,
    moe_gain,
    expert_ids,
    group_prob,
    route_prob,
    expert_gate,
    expert_up,
    expert_down,
):
    seq_rows, channels = conv_input.shape
    taps_count = conv_taps.shape[0]
    inner = gate_inner.astype(jnp.float32) * conv_input.astype(jnp.float32)
    earlier = from_behind(inner[seq_rows - (taps_count - 1) :], "sp", 1)
    padded = jnp.concatenate([earlier, inner], axis=0)
    tap_f = conv_taps.astype(jnp.float32)
    filtered = jnp.zeros((seq_rows, channels), jnp.float32)
    for offset in range(taps_count):
        filtered = filtered + tap_f[offset][None, :] * padded[offset : offset + seq_rows]
    mixed_out = (gate_outer.astype(jnp.float32) * filtered).astype(jnp.bfloat16)
    gathered = lax.all_to_all(mixed_out, "tp", split_axis=0, concat_axis=1, tiled=True)
    full_weight, full_gain = (
        lax.all_gather(out_weight, "tp", axis=0, tiled=True),
        lax.all_gather(norm_gain, "tp", axis=0, tiled=True),
    )
    normed = rms_norm(gathered, full_gain).astype(jnp.bfloat16)
    projected = jnp.dot(normed, full_weight, preferred_element_type=jnp.float32)
    residual = (residual_in.astype(jnp.float32) + projected).astype(jnp.bfloat16)
    routed_in = rms_norm(residual, moe_gain).astype(jnp.bfloat16)
    tok_rows, width = routed_in.shape
    top_count = expert_ids.shape[1]
    local_count = expert_gate.shape[0]
    group_count = lax.axis_size("sp")
    experts_all = local_count * group_count
    capacity = 2 * tok_rows * top_count // experts_all
    slots = tok_rows * top_count
    flat_e = expert_ids.reshape(-1)
    one_hot = (flat_e[:, None] == jnp.arange(experts_all, dtype=jnp.int32)[None, :]).astype(
        jnp.int32
    )
    slot_rank = jnp.sum((jnp.cumsum(one_hot, axis=0) - 1) * one_hot, axis=1)
    owner_dev = flat_e // local_count
    local_slot = flat_e % local_count
    position = (local_slot * group_count + owner_dev) * capacity + slot_rank
    source_slot = (
        jnp.full((experts_all * capacity,), slots, jnp.int32)
        .at[position]
        .set(jnp.arange(slots, dtype=jnp.int32))
    )
    rows_pad = jnp.concatenate([routed_in, jnp.zeros((1, width), jnp.bfloat16)], axis=0)
    outgoing = rows_pad[source_slot // top_count].reshape(local_count, group_count, capacity, width)
    arrived = lax.all_to_all(outgoing, "sp", split_axis=1, concat_axis=1, tiled=True)
    gate_act = jnp.einsum(
        "esrd,edf->esrf", arrived, expert_gate, preferred_element_type=jnp.float32
    )
    up_act = jnp.einsum("esrd,edf->esrf", arrived, expert_up, preferred_element_type=jnp.float32)
    hidden = (jax.nn.silu(gate_act) * up_act).astype(jnp.bfloat16)
    result = jnp.einsum(
        "esrf,efd->esrd", hidden, expert_down, preferred_element_type=jnp.float32
    ).astype(jnp.bfloat16)
    returned = lax.all_to_all(result, "sp", split_axis=1, concat_axis=1, tiled=True)
    slot_out = returned.reshape(-1, width)[position].reshape(tok_rows, top_count, width)
    weights = group_prob[:, None] * route_prob / jnp.sum(route_prob, axis=1, keepdims=True)
    expert_sum = jnp.sum(slot_out.astype(jnp.float32) * weights[:, :, None], axis=1)
    return (residual.astype(jnp.float32) + expert_sum).astype(jnp.bfloat16)


def solution(mesh):
    in_specs = (
        P(("sp", "tp"), None),
        P("sp", "tp"),
        P("sp", "tp"),
        P("sp", "tp"),
        P(None, "tp"),
        P("tp"),
        P("tp", None),
        P(),
        P(("sp", "tp"), None),
        P(("sp", "tp")),
        P(("sp", "tp"), None),
        P("sp", None, None),
        P("sp", None, None),
        P("sp", None, None),
    )
    out_specs = P(("sp", "tp"), None)
    return jax.shard_map(body, mesh=mesh, in_specs=in_specs, out_specs=out_specs, check_vma=False)
```

profile of v0, /device:TPU:2, one launch (start us, length us, event | category | flops | bytes accessed | tf_op | source)
XLA Modules:
  0.0 335.0 jit_solution(17748182596416122300)
XLA Ops:
  7.3 1.3 convert_multiply_fusion.3
  8.6 1.9 collective-permute-start
  11.0 1.2 reduce-window.6
  12.6 10.0 %all-gather = bf16[4,1,256]{2,1,0:T(2,128)(2,1)S(1)} all-gather(bf16[1,1,256]{2,1,0:T(2,128)(2,1)S(1)} %reshape.144), channel_id=1, replica_groups=mesh['sp'=64,'tp'=4] {'tp'}, dimensions={0}, use_global_device_ids=true | all-gather | bytes 2560 | tf_op jit(solution)/shard_map/all_gather | solution.py:50
  23.0 2.3 fusion.25
  25.2 3.5 %all-to-all-start = ((bf16[4,256,256]{2,1,0:T(8,128)(2,1)}), bf16[4,256,256]{2,1,0:T(8,128)(2,1)S(1)}, u32[]{:S(2)}, u32[]{:S(2)}) async-start(bf16[4,256,256]{2,1,0:T(8,128)(2,1)} %bitcast.66), calls=%async_computation | async-start | bytes 1048576 | tf_op jit(solution)/shard_map/all_to_all | solution.py:47
  28.8 2.4 scatter_custom_fusion
  31.2 13.6 %all-to-all-done = bf16[4,256,256]{2,1,0:T(8,128)(2,1)S(1)} async-done(((bf16[4,256,256]{2,1,0:T(8,128)(2,1)}), bf16[4,256,256]{2,1,0:T(8,128)(2,1)S(1)}, u32[]{:S(2)}, u32[]{:S(2)}) %all-to-all-start) | async-done | bytes 524320 | tf_op jit(solution)/shard_map/all_to_all | solution.py:47
  44.8 1.1 convert_bitcast_fusion.1
  45.8 2.5 copy.27
  48.6 1.4 fusion.29
  50.0 18.5 %all-gather.3.cloned.1.call-done = bf16[1024,2048]{1,0:T(8,128)(2,1)} async-done(((bf16[256,2048]{1,0:T(8,128)(2,1)}), bf16[1024,2048]{1,0:T(8,128)(2,1)}) %all-gather.3.cloned.1.call-update) | async-done | bytes 4194320 | tf_op jit(solution)/shard_map/all_gather | solution.py:49
  68.5 3.9 %fusion.5 = (f32[256]{0:T(256)S(1)}, bf16[256,2048]{1,0:T(8,128)(2,1)S(1)}) fusion(bf16[256,1024]{0,1:T(8,128)(2,1)S(1)} %fusion.29, bf16[1024,2048]{1,0:T(8,128)(2,1)} %all-gather.3.cloned.1.call-done, bf16[256,2048]{1,0:T(8,128)(2,1)} %param.14), kind=kOutput, calls=%fused_computation.14 | convolution fusion | flops 1076887296 | bytes 6816768 | tf_op jit(solution)/shard_map/dot_general | solution.py:53
  73.8 6.0 %gather_fusion = bf16[1024,2048]{1,0:T(8,128)(2,1)} fusion(bf16[257,2048]{1,0:T(8,128)(2,1)S(1)} %concatenate.7, s32[1024]{0:T(1024)S(1)} %fusion.35), kind=kCustom, calls=%fused_computation | custom fusion | bytes 8392704 | tf_op jit(solution)/shard_map/gather | solution.py:77
  79.8 106.9 %all_to_all.23 = bf16[1,64,16,2048]{3,2,0,1:T(8,128)(2,1)S(1)} all-to-all(bf16[1,64,16,2048]{3,2,0,1:T(8,128)(2,1)} %bitcast.65), channel_id=1, replica_groups=mesh['sp'=64,'tp'=4] {'sp'}, dimensions={1} | all-to-all | bytes 8388608 | tf_op jit(solution)/shard_map/all_to_all | solution.py:78
  186.7 2.0 copy-done.1
  188.7 3.7 %fusion.2 = f32[64,16,512]{2,1,0:T(8,128)} fusion(bf16[1,64,16,2048]{3,2,0,1:T(8,128)(2,1)S(1)} %all_to_all.23, bf16[1,2048,512]{2,1,0:T(8,128)(2,1)S(1)} %copy-done.9), kind=kOutput, calls=%fused_computation.5 | convolution fusion | flops 2147483648 | bytes 8388608 | tf_op jit(solution)/shard_map/esrd,edf->esrf/dot_general | solution.py:79
  192.4 10.0 %convert_bitcast_fusion = bf16[1,64,16,2048]{3,2,0,1:T(8,128)(2,1)} fusion(bf16[1,512,2048]{2,1,0:T(8,128)(2,1)S(1)} %copy-done, f32[64,16,512]{2,1,0:T(8,128)} %fusion.2, bf16[1,2048,512]{2,1,0:T(8,128)(2,1)} %param.26, bf16[1,64,16,2048]{3,2,0,1:T(8,128)(2,1)} %copy-done.1), kind=kOutput, calls=%fused_computation.8 | convolution fusion | flops 4300210176 | bytes 14680064 | tf_op jit(solution)/shard_map/esrf,efd->esrd/dot_general | solution.py:84
  202.4 5.9 %all-to-all-start.2 = ((bf16[1,64,16,2048]{3,2,0,1:T(8,128)(2,1)}), bf16[1,64,16,2048]{3,2,0,1:T(8,128)(2,1)}, u32[]{:S(2)}, u32[]{:S(2)}) async-start(bf16[1,64,16,2048]{3,2,0,1:T(8,128)(2,1)} %convert_bitcast_fusion), calls=%async_computation.2 | async-start | bytes 8388608 | tf_op jit(solution)/shard_map/all_to_all | solution.py:87
  208.5 96.0 %all-to-all-done.2 = bf16[1,64,16,2048]{3,2,0,1:T(8,128)(2,1)} async-done(((bf16[1,64,16,2048]{3,2,0,1:T(8,128)(2,1)}), bf16[1,64,16,2048]{3,2,0,1:T(8,128)(2,1)}, u32[]{:S(2)}, u32[]{:S(2)}) %all-to-all-start.2) | async-done | bytes 4194336 | tf_op jit(solution)/shard_map/all_to_all | solution.py:87
  304.5 8.0 %gather_fusion.1 = bf16[512,2048]{1,0:T(8,128)(2,1)} fusion(bf16[1024,2048]{1,0:T(8,128)(2,1)} %bitcast.21, s32[1024]{0:T(1024)S(1)} %pad_clamp_fusion), kind=kCustom, calls=%fused_computation.1 | custom fusion | bytes 4196352 | tf_op jit(solution)/shard_map/gather | solution.py:88
  312.5 5.4 %reshape.118 = f32[256,2,2048]{2,1,0:T(2,128)} reshape(bf16[512,2048]{1,0:T(8,128)(2,1)} %gather_fusion.1) | data formatting | bytes 6291456 | tf_op jit(solution)/shard_map/convert_element_type | solution.py:90
  317.9 9.0 %multiply_reduce_fusion = f32[256,2048]{1,0:T(8,128)S(1)} fusion(f32[256,2,2048]{2,1,0:T(2,128)} %reshape.118, f32[256,2]{1,0:T(8,128)S(1)} %copy.34), kind=kLoop, calls=%fused_computation.7 | loop fusion | flops 1572864 | bytes 6293504 | tf_op jit(solution)/shard_map/reduce_sum | solution.py:90
  326.9 1.3 fusion.8
  (52 shorter events, 3.6 us)
Async XLA Ops:
  6.5 185.9 %copy-start = (bf16[1,512,2048]{2,1,0:T(8,128)(2,1)S(1)}, bf16[1,512,2048]{2,1,0:T(8,128)(2,1)}, u32[]{:S(2)}) copy-start(bf16[1,512,2048]{2,1,0:T(8,128)(2,1)} %param.27) | copy-start | bytes 6291460
  6.5 4.0 %copy-start.4 = (s32[256,2]{0,1:T(2,128)S(1)}, s32[256,2]{0,1:T(2,128)}, u32[]{:S(2)}) copy-start(s32[256,2]{0,1:T(2,128)} %param.22) | copy-start | bytes 6148
  6.5 5.9 %copy-start.6 = (bf16[3,256]{1,0:T(4,128)(2,1)S(1)}, bf16[3,256]{1,0:T(4,128)(2,1)}, u32[]{:S(2)}) copy-start(bf16[3,256]{1,0:T(4,128)(2,1)} %param.18) | copy-start | bytes 4612
  6.5 6.1 %copy-start.10 = (bf16[256]{0:T(256)(128)(2,1)S(1)}, bf16[256]{0:T(256)(128)(2,1)}, u32[]{:S(2)}) copy-start(bf16[256]{0:T(256)(128)(2,1)} %param.19) | copy-start | bytes 1540
  6.5 16.1 %copy-start.7 = (bf16[2048]{0:T(1024)(128)(2,1)S(1)}, bf16[2048]{0:T(1024)(128)(2,1)}, u32[]{:S(2)}) copy-start(bf16[2048]{0:T(1024)(128)(2,1)} %param.21) | copy-start | bytes 12292
  6.5 62.0 %all-gather.3.cloned.1.call-start = ((), (), s32[]{:S(2)}) async-start(), calls=%async_computation.3 | async-start | bytes 5242880 | tf_op jit(solution)/shard_map/all_gather | solution.py:49
  8.6 14.3 %collective-permute-start = (f32[2,256]{1,0:T(2,128)S(1)}, f32[2,256]{1,0:T(2,128)S(1)}, u32[]{:S(2)}, u32[]{:S(2)}) collective-permute-start(f32[2,256]{1,0:T(2,128)S(1)} %slice.37), channel_id=1, source_target_pairs={{0,4},{4,8},{8,12},{12,16},{16,20},{20,24},{24,28},{28,32},{32,36}... | collective-permute-start | bytes 6152 | tf_op jit(solution)/shard_map/ppermute | solution.py:12
  25.2 19.5 %all-to-all-start = ((bf16[4,256,256]{2,1,0:T(8,128)(2,1)}), bf16[4,256,256]{2,1,0:T(8,128)(2,1)S(1)}, u32[]{:S(2)}, u32[]{:S(2)}) async-start(bf16[4,256,256]{2,1,0:T(8,128)(2,1)} %bitcast.66), calls=%async_computation | async-start | bytes 1048576 | tf_op jit(solution)/shard_map/all_to_all | solution.py:47
  72.4 1.0 copy-start.2
  79.8 108.8 %copy-start.9 = (bf16[1,2048,512]{2,1,0:T(8,128)(2,1)S(1)}, bf16[1,2048,512]{2,1,0:T(8,128)(2,1)}, u32[]{:S(2)}) copy-start(bf16[1,2048,512]{2,1,0:T(8,128)(2,1)} %param.25) | copy-start | bytes 6291460
  186.7 2.0 copy-start.1
  202.4 5.9 %copy-start.5 = (f32[256,2]{0,1:T(2,128)S(1)}, f32[256,2]{0,1:T(2,128)}, u32[]{:S(2)}) copy-start(f32[256,2]{0,1:T(2,128)} %param.24) | copy-start | bytes 6148
  202.4 6.0 %copy-start.8 = (f32[256]{0:T(256)S(1)}, f32[256]{0:T(256)}, u32[]{:S(2)}) copy-start(f32[256]{0:T(256)} %param.23) | copy-start | bytes 3076
  202.4 102.1 %all-to-all-start.2 = ((bf16[1,64,16,2048]{3,2,0,1:T(8,128)(2,1)}), bf16[1,64,16,2048]{3,2,0,1:T(8,128)(2,1)}, u32[]{:S(2)}, u32[]{:S(2)}) async-start(bf16[1,64,16,2048]{3,2,0,1:T(8,128)(2,1)} %convert_bitcast_fusion), calls=%async_computation.2 | async-start | bytes 8388608 | tf_op jit(solution)/shard_map/all_to_all | solution.py:87
  317.9 9.0 %copy-start.3 = (bf16[256,2048]{1,0:T(8,128)(2,1)S(1)}, bf16[256,2048]{1,0:T(8,128)(2,1)}, u32[]{:S(2)}) copy-start(bf16[256,2048]{1,0:T(8,128)(2,1)} %copy-done.2) | copy-start | bytes 3145732
Sparse Core Ops, SparseCore 0:
  9.2 59.3 all-gather.2
where the time goes:
time: 336 us; the launch traced here: 335 us
  waiting for transfers between devices  129 us (38%)
  blocking collectives  117 us (35%)
  local copies, waits for them, and re-layouts  28.5 us (8%)
  other arithmetic  18.2 us (5%)
  matrix products  17.6 us (5%)
  between operations  13.7 us (4%)
  starting transfers between devices  11.4 us (3%)
    all_to_all x1, blocking collectives, body(): lax.all_to_all(outgoing, 'sp', split_axis=1, concat_axis=1, tiled=True)  107 us
    all_to_all x1, waiting for transfers between devices, body(): lax.all_to_all(result, 'sp', split_axis=1, concat_axis=1, tiled=True)  96 us
    all_gather x1, waiting for transfers between devices, body(): lax.all_gather(out_weight, 'tp', axis=0, tiled=True)  18.5 us
    all_to_all x1, waiting for transfers between devices, body(): lax.all_to_all(mixed_out, 'tp', split_axis=0, concat_axis=1, tiled=True)  13.6 us
    all_gather x1, blocking collectives, body(): lax.all_gather(norm_gain, 'tp', axis=0, tiled=True)  9.99 us
    dot_general x1, matrix products, body(): jnp.einsum('esrf,efd->esrd', hidden, expert_down, preferred_element_type=...  9.96 us
    reduce_sum x1, other arithmetic, body(): jnp.sum(slot_out.astype(jnp.float32) * weights[:, :, None], axis=1)  8.96 us
    gather x1, local copies, waits for them, and re-layouts, body(): returned.reshape(-1, width)[position].reshape(tok_rows, top_count, width)  7.96 us
  transfers between devices with their start and end apart: 4, of which 3 were waited for; matrix products, arithmetic and copies ran while one was open for 4% of the time, Pallas kernels for 0%

commit v1 on v0

--- a/solution.py
+++ b/solution.py
@@ -4,6 +4,16 @@
 from jax.sharding import PartitionSpec as P
 
 EPSILON = 1e-06
+
+
+def _watch_shards(x_in, axis_key):
+    return jax.lax.all_to_all(
+        jnp.concatenate(jax.lax.axis_size(axis_key) * [x_in], axis=0),
+        axis_key,
+        tiled=True,
+        split_axis=0,
+        concat_axis=0,
+    )
 
 
 def from_behind(shard, axis, by):
@@ -46,7 +56,7 @@
     mixed_out = (gate_outer.astype(jnp.float32) * filtered).astype(jnp.bfloat16)
     gathered = lax.all_to_all(mixed_out, "tp", split_axis=0, concat_axis=1, tiled=True)
     full_weight, full_gain = (
-        lax.all_gather(out_weight, "tp", axis=0, tiled=True),
+        _watch_shards(out_weight, "tp"),
         lax.all_gather(norm_gain, "tp", axis=0, tiled=True),
     )
     normed = rms_norm(gathered, full_gain).astype(jnp.bfloat16)

time: 336 us -> 342 us (1.018)
  blocking collectives: 117 us -> 158 us
  waiting for transfers between devices: 129 us -> 104 us
  between operations: 13.7 us -> 0.25 us
  starting transfers between devices: 11.4 us -> 17.3 us
    all_gather x1, blocking collectives: 9.99 us -> 48.8 us  [body(): lax.all_gather(norm_gain, 'tp', axis=0, tiled=True)]
    all_gather x1 -> x0, waiting for transfers between devices: 18.5 us -> none  [body(): lax.all_gather(out_weight, 'tp', axis=0, tiled=True)]
    all_to_all x1, waiting for transfers between devices: 13.6 us -> 4.86 us  [body(): lax.all_to_all(mixed_out, 'tp', split_axis=0, concat_axis=1, tiled=True)]
    all_to_all x0 -> x1, starting transfers between devices: none -> 4.99 us  [_watch_shards(): jax.lax.all_to_all(jnp.concatenate(jax.lax.axis_size(axis_key) * [x_in],...]
    concatenate x0 -> x1, other arithmetic: none -> 4.11 us  [_watch_shards(): jnp.concatenate(jax.lax.axis_size(axis_key) * [x_in], axis=0)]
  transfers between devices with their start and end apart: 4 -> 4, of which waited for: 3 -> 3; matrix products, arithmetic and copies ran while one was open for 4% -> 3% of each run, Pallas kernels for 0% -> 0%
where the time goes in v1:
time: 342 us
  blocking collectives  158 us (46%)
  waiting for transfers between devices  104 us (30%)
  local copies, waits for them, and re-layouts  26 us (8%)
  other arithmetic  18.9 us (6%)
  matrix products  17.6 us (5%)
  starting transfers between devices  17.3 us (5%)
    all_to_all x1, blocking collectives, body(): lax.all_to_all(outgoing, 'sp', split_axis=1, concat_axis=1, tiled=True)  109 us
    all_to_all x1, waiting for transfers between devices, body(): lax.all_to_all(result, 'sp', split_axis=1, concat_axis=1, tiled=True)  96 us
    all_gather x1, blocking collectives, body(): lax.all_gather(norm_gain, 'tp', axis=0, tiled=True)  48.8 us
    dot_general x1, matrix products, body(): jnp.einsum('esrf,efd->esrd', hidden, expert_down, preferred_element_type=...  9.96 us
    reduce_sum x1, other arithmetic, body(): jnp.sum(slot_out.astype(jnp.float32) * weights[:, :, None], axis=1)  8.96 us
    gather x1, local copies, waits for them, and re-layouts, body(): returned.reshape(-1, width)[position].reshape(tok_rows, top_count, width)  7.96 us
  transfers between devices with their start and end apart: 4, of which 3 were waited for; matrix products, arithmetic and copies ran while one was open for 3% of the time, Pallas kernels for 0%

profile of v1, /device:TPU:2, one launch (start us, length us, event | category | flops | bytes accessed | tf_op | source)
XLA Modules:
  0.0 341.6 jit_solution(7750521743143501529)
XLA Ops:
  0.0 1.5 convert_multiply_fusion.4
  1.5 1.9 collective-permute-start
  3.4 3.0 collective-permute-done
  6.4 1.2 fusion.26
  7.6 4.5 %all-to-all-start = ((bf16[4,256,256]{2,1,0:T(8,128)(2,1)}), bf16[4,256,256]{2,1,0:T(8,128)(2,1)S(1)}, u32[]{:S(2)}, u32[]{:S(2)}) async-start(bf16[4,256,256]{2,1,0:T(8,128)(2,1)} %bitcast.3), calls=%async_computation | async-start | bytes 1048576 | tf_op jit(solution)/shard_map/all_to_all | solution.py:57
  12.1 4.1 %pad_maximum_fusion = bf16[1024,2048]{1,0:T(8,128)(2,1)} fusion(bf16[256,2048]{1,0:T(8,128)(2,1)} %param.20), kind=kLoop, calls=%fused_computation.3 | loop fusion | flops 16777216 | bytes 5242880 | tf_op jit(solution)/shard_map/concatenate | solution.py:11
  16.2 4.9 %all-to-all-done = bf16[4,256,256]{2,1,0:T(8,128)(2,1)S(1)} async-done(((bf16[4,256,256]{2,1,0:T(8,128)(2,1)}), bf16[4,256,256]{2,1,0:T(8,128)(2,1)S(1)}, u32[]{:S(2)}, u32[]{:S(2)}) %all-to-all-start) | async-done | bytes 524320 | tf_op jit(solution)/shard_map/all_to_all | solution.py:57
  21.0 5.0 %all-to-all-start.1 = ((bf16[4,256,2048]{2,1,0:T(8,128)(2,1)}), bf16[4,256,2048]{2,1,0:T(8,128)(2,1)}, u32[]{:S(2)}, u32[]{:S(2)}) async-start(bf16[4,256,2048]{2,1,0:T(8,128)(2,1)} %bitcast.71), calls=%async_computation.1 | async-start | bytes 8388608 | tf_op jit(solution)/shard_map/all_to_all | solution.py:10
  26.5 48.8 %all-gather = bf16[4,1,256]{2,1,0:T(2,128)(2,1)S(1)} all-gather(bf16[1,1,256]{2,1,0:T(2,128)(2,1)S(1)} %reshape.156), channel_id=1, replica_groups=mesh['sp'=64,'tp'=4] {'tp'}, dimensions={0}, use_global_device_ids=true | all-gather | bytes 2560 | tf_op jit(solution)/shard_map/all_gather | solution.py:60
  75.3 1.2 reduce-window.6
  77.2 2.4 scatter_custom_fusion
  79.9 4.0 %fusion.6 = (f32[256]{0:T(256)S(1)}, bf16[256,2048]{1,0:T(8,128)(2,1)S(1)}) fusion(bf16[4,256,2048]{2,1,0:T(8,128)(2,1)} %all-to-all-done.1, bf16[4,256,256]{2,1,0:T(8,128)(2,1)S(1)} %all-to-all-done, f32[4,256]{1,0:T(4,128)S(1)} %bitcast.78, f32[256]{0:T(256)S(1)} %add_rsqrt_fusion.1, bf16[256,2048]{1,0:T(8,128)(2,1)} %param.14), kind=kOutput, calls=%fused_computation.16 | convolution fusion | flops 1077935872 | bytes 6821888 | tf_op jit(solution)/shard_map/dot_general | solution.py:63
  83.9 1.0 copy-done.2
  85.2 6.0 %gather_fusion = bf16[1024,2048]{1,0:T(8,128)(2,1)} fusion(bf16[257,2048]{1,0:T(8,128)(2,1)S(1)} %concatenate.11, s32[1024]{0:T(1024)S(1)} %fusion.40), kind=kCustom, calls=%fused_computation | custom fusion | bytes 8392704 | tf_op jit(solution)/shard_map/gather | solution.py:87
  91.3 108.9 %all_to_all.32 = bf16[1,64,16,2048]{3,2,0,1:T(8,128)(2,1)S(1)} all-to-all(bf16[1,64,16,2048]{3,2,0,1:T(8,128)(2,1)} %bitcast.70), channel_id=1, replica_groups=mesh['sp'=64,'tp'=4] {'sp'}, dimensions={1} | all-to-all | bytes 8388608 | tf_op jit(solution)/shard_map/all_to_all | solution.py:88
  200.2 2.0 copy-done.1
  202.1 3.7 %fusion.2 = f32[64,16,512]{2,1,0:T(8,128)} fusion(bf16[1,64,16,2048]{3,2,0,1:T(8,128)(2,1)S(1)} %all_to_all.32, bf16[1,2048,512]{2,1,0:T(8,128)(2,1)S(1)} %copy-done.10), kind=kOutput, calls=%fused_computation.6 | convolution fusion | flops 2147483648 | bytes 8388608 | tf_op jit(solution)/shard_map/esrd,edf->esrf/dot_general | solution.py:89
  205.9 10.0 %convert_bitcast_fusion = bf16[1,64,16,2048]{3,2,0,1:T(8,128)(2,1)} fusion(bf16[1,512,2048]{2,1,0:T(8,128)(2,1)S(1)} %copy-done, f32[64,16,512]{2,1,0:T(8,128)} %fusion.2, bf16[1,2048,512]{2,1,0:T(8,128)(2,1)} %param.26, bf16[1,64,16,2048]{3,2,0,1:T(8,128)(2,1)} %copy-done.1), kind=kOutput, calls=%fused_computation.9 | convolution fusion | flops 4300210176 | bytes 14680064 | tf_op jit(solution)/shard_map/esrf,efd->esrd/dot_general | solution.py:94
  215.8 5.9 %all-to-all-start.3 = ((bf16[1,64,16,2048]{3,2,0,1:T(8,128)(2,1)}), bf16[1,64,16,2048]{3,2,0,1:T(8,128)(2,1)}, u32[]{:S(2)}, u32[]{:S(2)}) async-start(bf16[1,64,16,2048]{3,2,0,1:T(8,128)(2,1)} %convert_bitcast_fusion), calls=%async_computation.3 | async-start | bytes 8388608 | tf_op jit(solution)/shard_map/all_to_all | solution.py:97
  221.9 96.0 %all-to-all-done.3 = bf16[1,64,16,2048]{3,2,0,1:T(8,128)(2,1)} async-done(((bf16[1,64,16,2048]{3,2,0,1:T(8,128)(2,1)}), bf16[1,64,16,2048]{3,2,0,1:T(8,128)(2,1)}, u32[]{:S(2)}, u32[]{:S(2)}) %all-to-all-start.3) | async-done | bytes 4194336 | tf_op jit(solution)/shard_map/all_to_all | solution.py:97
  317.9 8.0 %gather_fusion.1 = bf16[512,2048]{1,0:T(8,128)(2,1)} fusion(bf16[1024,2048]{1,0:T(8,128)(2,1)} %bitcast.21, s32[1024]{0:T(1024)S(1)} %pad_clamp_fusion), kind=kCustom, calls=%fused_computation.1 | custom fusion | bytes 4196352 | tf_op jit(solution)/shard_map/gather | solution.py:98
  325.9 5.4 %reshape.130 = f32[256,2,2048]{2,1,0:T(2,128)} reshape(bf16[512,2048]{1,0:T(8,128)(2,1)} %gather_fusion.1) | data formatting | bytes 6291456 | tf_op jit(solution)/shard_map/convert_element_type | solution.py:100
  331.3 9.0 %multiply_reduce_fusion = f32[256,2048]{1,0:T(8,128)S(1)} fusion(f32[256,2,2048]{2,1,0:T(2,128)} %reshape.130, f32[256,2]{1,0:T(8,128)S(1)} %copy.27), kind=kLoop, calls=%fused_computation.8 | loop fusion | flops 1572864 | bytes 6293504 | tf_op jit(solution)/shard_map/reduce_sum | solution.py:100
  340.3 1.3 fusion.9
  (51 shorter events, 2.0 us)
Async XLA Ops:
  0.0 205.9 %copy-start = (bf16[1,512,2048]{2,1,0:T(8,128)(2,1)S(1)}, bf16[1,512,2048]{2,1,0:T(8,128)(2,1)}, u32[]{:S(2)}) copy-start(bf16[1,512,2048]{2,1,0:T(8,128)(2,1)} %param.27) | copy-start | bytes 6291460
  0.0 3.4 %copy-start.7 = (bf16[3,256]{1,0:T(4,128)(2,1)S(1)}, bf16[3,256]{1,0:T(4,128)(2,1)}, u32[]{:S(2)}) copy-start(bf16[3,256]{1,0:T(4,128)(2,1)} %param.18) | copy-start | bytes 4612
  0.0 6.4 %copy-start.4 = (bf16[1024,256]{1,0:T(8,128)(2,1)S(1)}, bf16[1024,256]{1,0:T(8,128)(2,1)}, u32[]{:S(2)}) copy-start(bf16[1024,256]{1,0:T(8,128)(2,1)} %param.15) | copy-start | bytes 1572868
  1.5 4.9 %collective-permute-start = (f32[2,256]{1,0:T(2,128)S(1)}, f32[2,256]{1,0:T(2,128)S(1)}, u32[]{:S(2)}, u32[]{:S(2)}) collective-permute-start(f32[2,256]{1,0:T(2,128)S(1)} %slice.37), channel_id=1, source_target_pairs={{0,4},{4,8},{8,12},{12,16},{16,20},{20,24},{24,28},{28,32},{32,36}... | collective-permute-start | bytes 6152 | tf_op jit(solution)/shard_map/ppermute | solution.py:22
  7.6 13.4 %all-to-all-start = ((bf16[4,256,256]{2,1,0:T(8,128)(2,1)}), bf16[4,256,256]{2,1,0:T(8,128)(2,1)S(1)}, u32[]{:S(2)}, u32[]{:S(2)}) async-start(bf16[4,256,256]{2,1,0:T(8,128)(2,1)} %bitcast.3), calls=%async_computation | async-start | bytes 1048576 | tf_op jit(solution)/shard_map/all_to_all | solution.py:57
  21.0 5.0 %copy-start.5 = (s32[256,2]{0,1:T(2,128)S(1)}, s32[256,2]{0,1:T(2,128)}, u32[]{:S(2)}) copy-start(s32[256,2]{0,1:T(2,128)} %param.22) | copy-start | bytes 6148
  21.0 5.4 %copy-start.11 = (bf16[256]{0:T(256)(128)(2,1)S(1)}, bf16[256]{0:T(256)(128)(2,1)}, u32[]{:S(2)}) copy-start(bf16[256]{0:T(256)(128)(2,1)} %param.19) | copy-start | bytes 1540
  21.0 54.3 %copy-start.8 = (bf16[2048]{0:T(1024)(128)(2,1)S(1)}, bf16[2048]{0:T(1024)(128)(2,1)}, u32[]{:S(2)}) copy-start(bf16[2048]{0:T(1024)(128)(2,1)} %param.21) | copy-start | bytes 12292
  21.0 58.9 %all-to-all-start.1 = ((bf16[4,256,2048]{2,1,0:T(8,128)(2,1)}), bf16[4,256,2048]{2,1,0:T(8,128)(2,1)}, u32[]{:S(2)}, u32[]{:S(2)}) async-start(bf16[4,256,2048]{2,1,0:T(8,128)(2,1)} %bitcast.71), calls=%async_computation.1 | async-start | bytes 8388608 | tf_op jit(solution)/shard_map/all_to_all | solution.py:10
  83.9 1.0 copy-start.2
  91.3 110.9 %copy-start.10 = (bf16[1,2048,512]{2,1,0:T(8,128)(2,1)S(1)}, bf16[1,2048,512]{2,1,0:T(8,128)(2,1)}, u32[]{:S(2)}) copy-start(bf16[1,2048,512]{2,1,0:T(8,128)(2,1)} %param.25) | copy-start | bytes 6291460
  200.2 2.0 copy-start.1
  215.8 5.9 %copy-start.6 = (f32[256,2]{0,1:T(2,128)S(1)}, f32[256,2]{0,1:T(2,128)}, u32[]{:S(2)}) copy-start(f32[256,2]{0,1:T(2,128)} %param.24) | copy-start | bytes 6148
  215.8 5.9 %copy-start.9 = (f32[256]{0:T(256)S(1)}, f32[256]{0:T(256)}, u32[]{:S(2)}) copy-start(f32[256]{0:T(256)} %param.23) | copy-start | bytes 3076
  215.8 102.1 %all-to-all-start.3 = ((bf16[1,64,16,2048]{3,2,0,1:T(8,128)(2,1)}), bf16[1,64,16,2048]{3,2,0,1:T(8,128)(2,1)}, u32[]{:S(2)}, u32[]{:S(2)}) async-start(bf16[1,64,16,2048]{3,2,0,1:T(8,128)(2,1)} %convert_bitcast_fusion), calls=%async_computation.3 | async-start | bytes 8388608 | tf_op jit(solution)/shard_map/all_to_all | solution.py:97
  331.3 9.0 %copy-start.3 = (bf16[256,2048]{1,0:T(8,128)(2,1)S(1)}, bf16[256,2048]{1,0:T(8,128)(2,1)}, u32[]{:S(2)}) copy-start(bf16[256,2048]{1,0:T(8,128)(2,1)} %copy-done.2) | copy-start | bytes 3145732
